TPU v7x, 256 devices: a whole 4x4x8 slice. The times are simulated.
256 devices in a mesh: sp: 32 (over z, y), tp: 8 (over x, core).
Axes of the slice: x: 4, y: 4, z: 8, core: 2. Of those that a mesh axis runs over, the one named last changes fastest.
Arguments:
- tokens: bfloat16 [4, 16384, 2048], P(None, ('sp', 'tp')), may hold values from -6 to 6
- in_gain: float32 [2048], replicated, may hold values from 0.1 to 1.9
- query_weight: bfloat16 [2048, 1024], P(None, 'tp'), may hold values from -0.125 to 0.125
- key_weight: bfloat16 [2048, 1024], P(None, 'tp'), may hold values from -0.125 to 0.125
- value_weight: bfloat16 [2048, 1024], P(None, 'tp'), may hold values from -0.125 to 0.125
- gate_weight: bfloat16 [2048, 1024], P(None, 'tp'), may hold values from -0.125 to 0.125
- log_decay: float32 [8], P('tp'), may hold values from -0.034 to 0, as said below
- norm_gain: float32 [1024], P('tp'), may hold values from 0.1 to 1.9
- out_weight: bfloat16 [1024, 2048], replicated, may hold values from -0.1875 to 0.1875
- post_gain: float32 [2048], replicated, may hold values from 0.1 to 1.9
Outputs:
- mixed: bfloat16 [4, 16384, 2048], P(None, ('sp', 'tp'))
Inputs may be any that keep to these rules, and one draw needn't show every extreme that they name: `log_decay`: every entry is negative; some heads keep a tenth or more of their memory over 16384 positions, others lose most of it within 30 to 100 positions.
All inputs are finite; a program needn't handle non-finite values.
Results may differ from a plain program's by a relative error of at most 0.015.
Values may be sent and summed in bfloat16 or wider, within the bound.
A program may use at most 64 MiB of HBM per device.

v0:
```python
import jax
import jax.numpy as jnp
from jax import lax
from jax.sharding import Mesh
from jax.sharding import PartitionSpec as P

HEAD_DIM = 128
BLOCK = 128
SP = ("sp_0", "sp_1")
SP_TP = ("sp_0", "sp_1", "tp")
rms_eps = 1e-06
group_eps = 1e-05
rope_base = 10000.0


def neutral_like(shard, identity):
    return jax.tree.map(
        lambda part, zero: jnp.zeros_like(part) + jnp.asarray(zero, part.dtype), shard, identity
    )


def entering(shard, axes, combine, identity):
    before = start = neutral_like(shard, identity)
    running = shard
    for axis in reversed(axes):
        length, mine = (lax.axis_size(axis), lax.axis_index(axis))
        pieces = jax.tree.map(lambda part: lax.all_gather(part, axis), running)
        inside, running = (start, start)
        for k in range(length):
            passed = k < mine
            running = combine(running, jax.tree.map(lambda part: part[k], pieces))
            inside = jax.tree.map(lambda new, old: jnp.where(passed, new, old), running, inside)
        before = combine(inside, before)
    return before


def rotate(values, positions):
    half_dim = values.shape[-1] // 2
    inverse = rope_base ** (-jnp.arange(half_dim, dtype=jnp.float32) / half_dim)
    angles = positions.astype(jnp.float32)[:, None] * inverse[None, :]
    cosine = jnp.cos(angles)
    sine_part = jnp.sin(angles)
    first_half = values[..., :half_dim].astype(jnp.float32)
    second = values[..., half_dim:].astype(jnp.float32)
    return jnp.concatenate(
        [first_half * cosine - second * sine_part, first_half * sine_part + second * cosine],
        axis=-1,
    )


def local_pass(queries, key_rows, values, log_decay):
    seq_count, head_count, length, head_width = queries.shape
    block_count = length // BLOCK
    offsets = jnp.arange(BLOCK, dtype=jnp.float32)
    distance = offsets[:, None] - offsets[None, :]
    rate_col = log_decay[:, None, None]
    inside = jnp.where(distance >= 0, jnp.exp(rate_col * jnp.maximum(distance, 0.0)), 0.0)
    query_scale = jnp.exp(log_decay[:, None] * (offsets + 1.0))[..., None]
    key_scale = jnp.exp(log_decay[:, None] * (BLOCK - 1.0 - offsets))[..., None]
    block_decay = jnp.exp(log_decay * BLOCK)[:, None, None]

    def to_blocks(arr):
        return arr.reshape(seq_count, head_count, block_count, BLOCK, arr.shape[-1]).transpose(
            2, 0, 1, 3, 4
        )

    def advance(memory, inputs):
        q_block, k_block, v_block = inputs
        scores = jnp.einsum("shqd,shkd->shqk", q_block, k_block, preferred_element_type=jnp.float32)
        weights = (scores * inside).astype(jnp.bfloat16)
        within = jnp.einsum("shqk,shkv->shqv", weights, v_block, preferred_element_type=jnp.float32)
        carried = jnp.einsum("shqd,shdv->shqv", q_block.astype(jnp.float32) * query_scale, memory)
        k_scaled = (k_block.astype(jnp.float32) * key_scale).astype(jnp.bfloat16)
        memory = memory * block_decay + jnp.einsum(
            "shkd,shkv->shdv", k_scaled, v_block, preferred_element_type=jnp.float32
        )
        return (memory, within + carried)

    start_memory = jnp.zeros((seq_count, head_count, head_width, values.shape[-1]), jnp.float32)
    end_state, outputs = lax.scan(
        advance, start_memory, (to_blocks(queries), to_blocks(key_rows), to_blocks(values))
    )
    outputs = outputs.transpose(1, 2, 0, 3, 4).reshape(
        seq_count, head_count, length, values.shape[-1]
    )
    return (outputs, end_state)


def combine(earlier, later_part):
    return (
        earlier[0] * later_part[0],
        earlier[1] * later_part[0][None, :, None, None] + later_part[1],
    )


def read_out(carried, queries, partial_out, log_decay):
    length = queries.shape[2]
    read_scale = jnp.exp(log_decay[:, None] * (jnp.arange(length, dtype=jnp.float32) + 1.0))[
        ..., None
    ]
    return partial_out + jnp.einsum(
        "shld,shdv->shlv", queries.astype(jnp.float32) * read_scale, carried
    )


def body(
    tokens,
    in_gain,
    query_weight,
    key_weight,
    value_weight,
    gate_weight,
    log_decay,
    norm_gain,
    out_weight,
    post_gain,
):
    seq_count, rows_dev, model_width = tokens.shape
    tp_size = lax.axis_size("tp")
    local_width = query_weight.shape[1]
    head_count = local_width // HEAD_DIM
    stretch = rows_dev * tp_size
    tok_f32 = tokens.astype(jnp.float32)
    normed = (
        tok_f32 * lax.rsqrt(jnp.mean(tok_f32 * tok_f32, axis=-1, keepdims=True) + rms_eps) * in_gain
    ).astype(jnp.bfloat16)
    joined = jnp.concatenate([query_weight, key_weight, value_weight, gate_weight], axis=1)
    projected = jnp.einsum(
        "kux,xt->kut",
        lax.all_gather(normed, "tp", axis=1, tiled=True),
        joined,
        preferred_element_type=jnp.float32,
    ).astype(jnp.bfloat16)

    def heads_of(columns):
        return columns.reshape(seq_count, stretch, head_count, HEAD_DIM).transpose(0, 2, 1, 3)

    positions = lax.axis_index(SP) * stretch + jnp.arange(stretch, dtype=jnp.int32)
    queries = rotate(heads_of(projected[..., :local_width]), positions).astype(jnp.bfloat16)
    key_rows = (
        rotate(heads_of(projected[..., local_width : 2 * local_width]), positions)
        * HEAD_DIM ** (-0.5)
    ).astype(jnp.bfloat16)
    values = heads_of(projected[..., 2 * local_width : 3 * local_width])
    gating = projected[..., 3 * local_width :]
    partial_out, end_state = local_pass(queries, key_rows, values, log_decay)
    span_decay = jnp.exp(log_decay * stretch)
    carried = entering(
        (span_decay, end_state), SP, combine, (jnp.ones_like(span_decay), jnp.zeros_like(end_state))
    )[1]
    retained = read_out(carried, queries, partial_out, log_decay)
    center = jnp.mean(retained, axis=-1, keepdims=True)
    spread = jnp.mean(jnp.square(retained - center), axis=-1, keepdims=True)
    normal = (
        ((retained - center) * lax.rsqrt(spread + group_eps))
        .transpose(0, 2, 1, 3)
        .reshape(seq_count, stretch, local_width)
    )
    gated = (normal * norm_gain * jax.nn.silu(gating.astype(jnp.float32))).astype(jnp.bfloat16)
    premix = jnp.einsum(
        "hor,rn->hon",
        lax.all_to_all(gated, "tp", split_axis=1, concat_axis=2, tiled=True),
        out_weight,
        preferred_element_type=jnp.float32,
    )
    mixed = (
        premix * lax.rsqrt(jnp.mean(premix * premix, axis=-1, keepdims=True) + rms_eps) * post_gain
    )
    return mixed.astype(jnp.bfloat16)


def solution(mesh):
    torus = Mesh(mesh.devices.reshape(8, 4, mesh.shape["tp"]), ("sp_0", "sp_1", "tp"))
    return jax.shard_map(
        body,
        mesh=torus,
        in_specs=(
            P(None, SP_TP, None),
            P(),
            P(None, "tp"),
            P(None, "tp"),
            P(None, "tp"),
            P(None, "tp"),
            P("tp"),
            P("tp"),
            P(),
            P(),
        ),
        out_specs=P(None, SP_TP, None),
        check_vma=False,
    )
```

profile of v0, /device:TPU:1, one launch (start us, length us, event | category | flops | bytes accessed | tf_op | source)
XLA Modules:
  0.0 204.7 jit_solution(9332395953188734523)
XLA Ops:
  6.5 1.6 fusion.44
  8.1 2.6 %fusion.46 = bf16[4,64,2048]{2,1,0:T(8,128)(2,1)} fusion(bf16[4,64,2048]{2,1,0:T(8,128)(2,1)} %param.12, f32[2048]{0:T(1024)} %param.13, f32[4,64]{1,0:T(4,128)S(1)} %add_rsqrt_fusion.2), kind=kLoop, calls=%fused_computation.48 | loop fusion | flops 2097152 | bytes 2106368 | tf_op jit(solution)/shard_map/convert_element_type | solution.py:126
  13.5 53.8 %all-gather.7.cloned.1.call-done = bf16[4,512,2048]{2,1,0:T(8,128)(2,1)} async-done(((bf16[4,64,2048]{2,1,0:T(8,128)(2,1)}), bf16[4,512,2048]{2,1,0:T(8,128)(2,1)}) %all-gather.7.cloned.1.call-update) | async-done | bytes 8388624 | tf_op jit(solution)/shard_map/all_gather | solution.py:130
  67.3 9.5 %fusion.54 = bf16[4,512,512]{1,2,0:T(8,128)(2,1)S(1)} fusion(bf16[4,512,2048]{2,1,0:T(8,128)(2,1)} %all-gather.7.cloned.1.call-done, bf16[2048,128]{0,1:T(8,128)(2,1)S(1)} %copy.42, bf16[2048,128]{0,1:T(8,128)(2,1)S(1)} %copy.41, bf16[2048,128]{0,1:T(8,128)(2,1)S(1)} %copy.40, bf16[2048,128]{0,1:T(8,128)(2,1)S(1)} %copy.39), kind=kOutput, calls=%fused_computation.59 | convolution fusion | flops 4304404480 | bytes 12582912 | tf_op jit(solution)/shard_map/kux,xt->kut/dot_general | solution.py:128
  76.9 1.0 slice_bitcast_fusion
  80.3 1.3 copy.44
  81.6 1.2 reshape_transpose_reshape.3
  83.5 0.9 copy-done.1
  84.8 11.9 %while.15 = (s32[]{:T(128)}, f32[4,1,128,128]{3,2,0,1:T(8,128)S(1)}, f32[4,4,1,128,128]{4,3,1,2,0:T(8,128)}, f32[1]{0:T(128)}, bf16[4,4,1,128,128]{4,3,1,2,0:T(8...) while((s32[]{:T(128)}, ...), condition=%wide.region_2.3_spmd.clone.clone.clone, body=%wide.region_1.2_spmd.clone.clone.clone.sunk | while | flops 67977728 | bytes 2496632 | solution.py:80
  84.8 0.7 select_bitcast_fusion.2
  86.5 0.9 fusion.147
  87.8 0.7 select_bitcast_fusion.2
  89.5 0.9 fusion.147
  90.8 0.7 select_bitcast_fusion.2
  92.5 0.9 fusion.147
  93.8 0.7 select_bitcast_fusion.2
  95.5 0.9 fusion.147
  96.8 0.7 copy-done
  98.8 8.4 %all-reduce = f32[4]{0:T(128)S(1)} all-reduce(f32[4]{0:T(128)S(1)} %exponential_dynamic-update-slice_fusion), channel_id=2, replica_groups=mesh['sp_0'=8,'sp_1'=4,'tp'=8] {'sp_1'}, use_global_device_ids=true, to_apply=%add | all-reduce | flops 4 | bytes 32
  107.2 0.7 slice_multiply_fusion.1
  107.9 1.3 slice_multiply_fusion
  109.9 12.2 %all-gather.11.cloned.1.call-done = f32[16,1,128,128]{3,2,1,0:T(8,128)} async-done(((f32[4,1,128,128]{3,2,1,0:T(8,128)}), f32[16,1,128,128]{3,2,1,0:T(8,128)}) %all-gather.11.cloned.1.call-update) | async-done | bytes 1048592 | tf_op jit(solution)/shard_map/all_gather | solution.py:27
  122.0 3.8 %slice_add_fusion.8 = f32[4,1,128,128]{3,2,1,0:T(8,128)} fusion(f32[16,1,128,128]{3,2,1,0:T(8,128)} %all-gather.11.cloned.1.call-done, f32[]{:T(128)} %bitcast.20, f32[]{:T(128)} %bitcast.18, f32[16,1,128,128]{3,2,0,1:T(8,128)} %bitcast.197, f32[]{:T(128)} %bitcast.16, f32[]{:T(128)} %bitcast.13), kind=kLoop, calls=%fused_computation.109 | loop fusion | flops 458752 | bytes 1310736 | tf_op jit(solution)/shard_map/add | solution.py:92
  126.4 1.3 dynamic-update-slice.1
  127.7 13.9 %all-reduce.1 = f32[8]{0:T(128)S(1)} all-reduce(f32[8]{0:T(128)S(1)} %dynamic-update-slice.1), channel_id=3, replica_groups=mesh['sp_0'=8,'sp_1'=4,'tp'=8] {'sp_0'}, use_global_device_ids=true, to_apply=%add.1 | all-reduce | flops 8 | bytes 64
  141.6 0.7 fusion.127
  146.3 18.7 %all-gather.9.cloned.1.call-done = f32[8,4,1,128,128]{4,3,2,1,0:T(8,128)} async-done(((f32[1,4,1,128,128]{4,3,2,1,0:T(8,128)}), f32[8,4,1,128,128]{4,3,2,1,0:T(8,128)}) %all-gather.9.cloned.1.call-update) | async-done | bytes 2097168 | tf_op jit(solution)/shard_map/all_gather | solution.py:27
  165.1 7.9 %fusion.128 = (f32[4,512]{1,0:T(4,128)S(1)}, f32[4,512,128]{1,2,0:T(8,128)S(1)}) fusion(f32[4,512,128]{1,2,0:T(8,128)S(1)} %reshape.499, f32[8,4,1,128,128]{4,3,1,2,0:T(8,128)} %bitcast.204, f32[4,1,128,128]{3,2,1,0:T(8,128)S(1)} %copy-done.4, f32[16,1,128,128]{3,2,0,1:T(8,128)S(1)} %bitcast.198, f32[16,1,128,128]{3,2,1,0:T(8,128)S(1)} %copy-done.3, ...), kind=kOutput, calls=%fused_computation.175 | convolution fusion | flops 71170048 | bytes 5777468 | tf_op jit(solution)/shard_map/shld,shdv->shlv/dot_general | solution.py:101
  173.2 1.5 fusion.62
  175.0 18.3 %all_to_all.18 = bf16[4,512,128]{2,0,1:T(4,128)(2,1)S(1)} all-to-all(bf16[4,512,128]{2,0,1:T(4,128)(2,1)S(1)} %copy.65), channel_id=1, replica_groups=mesh['sp_0'=8,'sp_1'=4,'tp'=8] {'tp'}, dimensions={1} | all-to-all | bytes 1048576 | tf_op jit(solution)/shard_map/all_to_all | solution.py:162
  193.4 3.6 %multiply_reduce_fusion = (f32[4,64]{1,0:T(4,128)S(1)}, f32[4,64,2048]{2,1,0:T(8,128)S(1)}) fusion(bf16[1024,2048]{1,0:T(8,128)(2,1)} %param.20, bf16[4,8,8,8,128]{4,3,2,1,0:T(8,128)(2,1)S(1)} %bitcast.203), kind=kOutput, calls=%fused_computation.58 | convolution fusion | flops 1074790144 | bytes 6816768 | tf_op jit(solution)/shard_map/hor,rn->hon/dot_general | solution.py:160
  197.0 1.2 multiply_convert_fusion.2
  (83 shorter events, 13.9 us)
Async XLA Ops:
  6.5 4.3 %copy-start.8 = (bf16[2048,128]{1,0:T(8,128)(2,1)S(1)}, bf16[2048,128]{1,0:T(8,128)(2,1)}, u32[]{:S(2)}) copy-start(bf16[2048,128]{1,0:T(8,128)(2,1)} %param.14) | copy-start | bytes 1572868
  6.5 60.8 %all-gather.7.cloned.1.call-start = ((), (), s32[]{:S(2)}) async-start(), calls=%async_computation.1 | async-start | bytes 9437184 | tf_op jit(solution)/shard_map/all_gather | solution.py:130
  8.1 3.0 %copy-start.9 = (bf16[2048,128]{1,0:T(8,128)(2,1)S(1)}, bf16[2048,128]{1,0:T(8,128)(2,1)}, u32[]{:S(2)}) copy-start(bf16[2048,128]{1,0:T(8,128)(2,1)} %param.15) | copy-start | bytes 1572868
  10.8 1.0 copy-start.10
  10.8 1.3 copy-start.11
  10.8 111.2 %all-gather.11.cloned.1.call-start = ((), (), s32[]{:S(2)}) async-start(), calls=%async_computation.3 | async-start | bytes 1310720 | tf_op jit(solution)/shard_map/all_gather | solution.py:27
  76.9 1.5 copy-start.2
  78.3 0.7 copy-start.6
  78.4 0.8 copy-start.7
  83.2 1.2 copy-start.1
  84.8 12.8 %copy-start.15 = (u32[256]{0:T(256)S(1)}, u32[256]{0:T(256)}, u32[]{:S(2)}) copy-start(u32[256]{0:T(256)} %constant.86) | copy-start | bytes 3076
  84.8 41.1 %copy-start.14 = (u32[256]{0:T(256)S(1)}, u32[256]{0:T(256)}, u32[]{:S(2)}) copy-start(u32[256]{0:T(256)} %constant.91) | copy-start | bytes 3076
  96.7 0.7 copy-start
  96.7 48.7 %copy-start.5 = (f32[4,4,1,128,128]{4,3,1,2,0:T(8,128)S(1)}, f32[4,4,1,128,128]{4,3,1,2,0:T(8,128)}, u32[]{:S(2)}) copy-start(f32[4,4,1,128,128]{4,3,1,2,0:T(8,128)} %get-tuple-element.58) | copy-start | bytes 3145732
  97.5 67.6 %all-gather.9.cloned.1.call-start = ((), (), s32[]{:S(2)}) async-start(), calls=%async_computation.2 | async-start | bytes 2359296 | tf_op jit(solution)/shard_map/all_gather | solution.py:27
  145.5 19.6 %copy-start.3 = (f32[16,1,128,128]{3,2,1,0:T(8,128)S(1)}, f32[16,1,128,128]{3,2,1,0:T(8,128)}, u32[]{:S(2)}) copy-start(f32[16,1,128,128]{3,2,1,0:T(8,128)} %all-gather.11.cloned.1.call-done) | copy-start | bytes 3145732
  145.5 19.6 %copy-start.4 = (f32[4,1,128,128]{3,2,1,0:T(8,128)S(1)}, f32[4,1,128,128]{3,2,1,0:T(8,128)}, u32[]{:S(2)}) copy-start(f32[4,1,128,128]{3,2,1,0:T(8,128)} %slice_add_fusion.8) | copy-start | bytes 786436
  165.1 8.1 %copy-start.13 = (f32[128]{0:T(128)S(1)}, f32[128]{0:T(128)}, u32[]{:S(2)}) copy-start(f32[128]{0:T(128)} %param.19) | copy-start | bytes 1540
  193.4 3.6 %copy-start.12 = (f32[2048]{0:T(1024)S(1)}, f32[2048]{0:T(1024)}, u32[]{:S(2)}) copy-start(f32[2048]{0:T(1024)} %param.21) | copy-start | bytes 24580
Sparse Core Ops, SparseCore 0:
  10.9 56.3 all-gather.6
  97.6 24.3 all-gather.10
  126.0 39.0 all-gather.8
where the time goes:
time: 205 us
  waiting for transfers between devices  84.8 us (41%)
  blocking collectives  40.6 us (20%)
  matrix products  27.4 us (13%)
  other arithmetic  20.4 us (10%)
  between operations  18 us (9%)
  local copies, waits for them, and re-layouts  13.3 us (6%)
    all_gather x1, waiting for transfers between devices, body(): lax.all_gather(normed, 'tp', axis=1, tiled=True)  53.8 us
    all_gather x2, waiting for transfers between devices, entering(): pieces = jax.tree.map(lambda part: lax.all_gather(part, axis), running)  30.9 us
    unnamed x2, blocking collectives  22.3 us
    all_to_all x1, blocking collectives, body(): lax.all_to_all(gated, 'tp', split_axis=1, concat_axis=2, tiled=True)  18.3 us
    dot_general x1, matrix products, body(): jnp.einsum('kux,xt->kut', lax.all_gather(normed, 'tp', axis=1, tiled=True...  9.51 us
    dot_general x1, matrix products, read_out(): jnp.einsum('shld,shdv->shlv', queries.astype(jnp.float32) * read_scale, c...  7.93 us
    unnamed x41, local copies, waits for them, and re-layouts  6.03 us
  transfers between devices with their start and end apart: 3, of which 3 were waited for; matrix products, arithmetic and copies ran while one was open for 4% of the time, Pallas kernels for 0%

commit v1 on v0

--- a/solution.py
+++ b/solution.py
@@ -11,6 +11,27 @@
 rms_eps = 1e-06
 group_eps = 1e-05
 rope_base = 10000.0
+
+
+def collect(array, axis, dim):
+    size, position, rows = (lax.axis_size(axis), lax.axis_index(axis), array.shape[dim])
+    forward = [(i, (i + 1) % size) for i in range(size)]
+    left = [(i, (i - 1) % size) for i in range(size)]
+    filled = jnp.zeros((*array.shape[:dim], size * rows, *array.shape[dim + 1 :]), array.dtype)
+    filled = lax.dynamic_update_slice_in_dim(filled, array, position * rows, axis=dim)
+    from_left = from_right = array
+    halfway = size // 2
+    for step in range(1, halfway + 1):
+        from_left = lax.ppermute(from_left, axis, forward)
+        filled = lax.dynamic_update_slice_in_dim(
+            filled, from_left, (position - step) % size * rows, axis=dim
+        )
+        if step < size - halfway:
+            from_right = lax.ppermute(from_right, axis, left)
+            filled = lax.dynamic_update_slice_in_dim(
+                filled, from_right, (position + step) % size * rows, axis=dim
+            )
+    return filled
 
 
 def neutral_like(shard, identity):
@@ -126,10 +147,7 @@
     ).astype(jnp.bfloat16)
     joined = jnp.concatenate([query_weight, key_weight, value_weight, gate_weight], axis=1)
     projected = jnp.einsum(
-        "kux,xt->kut",
-        lax.all_gather(normed, "tp", axis=1, tiled=True),
-        joined,
-        preferred_element_type=jnp.float32,
+        "kux,xt->kut", collect(normed, "tp", 1), joined, preferred_element_type=jnp.float32
     ).astype(jnp.bfloat16)
 
     def heads_of(columns):

time: 205 us -> 219 us (1.068)
  waiting for transfers between devices: 84.8 us -> 62 us
  local copies, waits for them, and re-layouts: 13.3 us -> 36 us
  starting transfers between devices: 0.09 us -> 12.8 us
    all_gather x1 -> x0, waiting for transfers between devices: 53.8 us -> none  [body(): lax.all_gather(normed, 'tp', axis=1, tiled=True)]
    ppermute x0 -> x7, waiting for transfers between devices: none -> 26.9 us  [the longest x4 23 us: collect(): from_left = lax.ppermute(from_left, axis, forward)]
    ppermute x0 -> x7, starting transfers between devices: none -> 12.7 us  [the longest x4 7.69 us: collect(): from_left = lax.ppermute(from_left, axis, forward)]
    dynamic_update_slice x0 -> x7, local copies, waits for them, and re-layouts: none -> 9.89 us  [the longest x4 6.75 us: collect(): lax.dynamic_update_slice_in_dim(filled, from_left, (position - step) % si...]
    unnamed x41, local copies, waits for them, and re-layouts: 6.03 us -> 13.4 us
    broadcast_in_dim x0 -> x1, local copies, waits for them, and re-layouts: none -> 4.32 us  [collect(): jnp.zeros((*array.shape[:dim], size * rows, *array.shape[dim + 1:]), arra...]
    all_gather x2, waiting for transfers between devices: 30.9 us -> 35.1 us  [entering(): pieces = jax.tree.map(lambda part: lax.all_gather(part, axis), running)]
    convert_element_type x1 -> x0, other arithmetic: 2.65 us -> none  [body(): normed = (tok_f32 * lax.rsqrt(jnp.mean(tok_f32 * tok_f32, axis=-1, keepdi...]
  transfers between devices with their start and end apart: 3 -> 9, of which waited for: 3 -> 7; matrix products, arithmetic and copies ran while one was open for 4% -> 12% of each run, Pallas kernels for 0% -> 0%
where the time goes in v1:
time: 219 us; the launch traced here: 218 us
  waiting for transfers between devices  62 us (28%)
  blocking collectives  40.7 us (19%)
  local copies, waits for them, and re-layouts  36 us (16%)
  matrix products  27.4 us (13%)
  other arithmetic  20.3 us (9%)
  between operations  18.3 us (8%)
  starting transfers between devices  12.8 us (6%)
    all_gather x2, waiting for transfers between devices, entering(): pieces = jax.tree.map(lambda part: lax.all_gather(part, axis), running)  35.1 us
    ppermute x4, waiting for transfers between devices, collect(): from_left = lax.ppermute(from_left, axis, forward)  23 us
    unnamed x2, blocking collectives  22.2 us
    all_to_all x1, blocking collectives, body(): lax.all_to_all(gated, 'tp', split_axis=1, concat_axis=2, tiled=True)  18.6 us
    unnamed x41, local copies, waits for them, and re-layouts  13.4 us
    dot_general x1, matrix products, body(): jnp.einsum('kux,xt->kut', collect(normed, 'tp', 1), joined, preferred_ele...  9.66 us
    dot_general x1, matrix products, read_out(): jnp.einsum('shld,shdv->shlv', queries.astype(jnp.float32) * read_scale, c...  7.81 us
    ppermute x4, starting transfers between devices, collect(): from_left = lax.ppermute(from_left, axis, forward)  7.69 us
  transfers between devices with their start and end apart: 9, of which 7 were waited for; matrix products, arithmetic and copies ran while one was open for 12% of the time, Pallas kernels for 0%

profile of v1, /device:TPU:1, one launch (start us, length us, event | category | flops | bytes accessed | tf_op | source)
XLA Modules:
  0.0 217.7 jit_solution(1565288610632173341)
XLA Ops:
  6.5 1.5 fusion.44
  8.1 4.3 %broadcast_in_dim.10 = bf16[4,512,2048]{2,1,0:T(8,128)(2,1)} broadcast(bf16[]{:T(256)} %constant.98.clone.1), dimensions={} | broadcast | bytes 8388610 | tf_op jit(solution)/shard_map/broadcast_in_dim | solution.py:20
  13.7 2.6 %collective-permute-start = (bf16[4,64,2048]{2,1,0:T(8,128)(2,1)S(1)}, bf16[4,64,2048]{2,1,0:T(8,128)(2,1)}, u32[]{:S(2)}, u32[]{:S(2)}) collective-permute-start(bf16[4,64,2048]{2,1,0:T(8,128)(2,1)S(1)} %get-tuple-element.162), channel_id=1, source_target_pairs={{0,1},{1,2},{2,3},{3,4},{4,5},{5,6},{6,7},{7,0},{8,9},{9,10},{10,1... | collective-permute-start | bytes 3145736 | tf_op jit(solution)/shard_map/ppermute | solution.py:25
  16.9 11.2 %collective-permute-done = bf16[4,64,2048]{2,1,0:T(8,128)(2,1)} collective-permute-done((bf16[4,64,2048]{2,1,0:T(8,128)(2,1)S(1)}, bf16[4,64,2048]{2,1,0:T(8,128)(2,1)}, u32[]{:S(2)}, u32[]{:S(2)}) %collective-permute-start) | collective-permute-done | bytes 1048608 | tf_op jit(solution)/shard_map/ppermute | solution.py:25
  28.1 2.6 %collective-permute-start.2 = (bf16[4,64,2048]{2,1,0:T(8,128)(2,1)}, bf16[4,64,2048]{2,1,0:T(8,128)(2,1)}, u32[]{:S(2)}, u32[]{:S(2)}) collective-permute-start(bf16[4,64,2048]{2,1,0:T(8,128)(2,1)} %collective-permute-done), channel_id=1, source_target_pairs={{0,1},{1,2},{2,3},{3,4},{4,5},{5,6},{6,7},{7,0},{8,9},{9,10},{10,1... | collective-permute-start | bytes 3145736 | tf_op jit(solution)/shard_map/ppermute | solution.py:25
  30.9 1.5 collective-permute-start.3
  32.4 10.3 %collective-permute-done.2 = bf16[4,64,2048]{2,1,0:T(8,128)(2,1)} collective-permute-done((bf16[4,64,2048]{2,1,0:T(8,128)(2,1)}, bf16[4,64,2048]{2,1,0:T(8,128)(2,1)}, u32[]{:S(2)}, u32[]{:S(2)}) %collective-permute-start.2) | collective-permute-done | bytes 1048608 | tf_op jit(solution)/shard_map/ppermute | solution.py:25
  42.7 2.5 %collective-permute-start.4 = (bf16[4,64,2048]{2,1,0:T(8,128)(2,1)}, bf16[4,64,2048]{2,1,0:T(8,128)(2,1)S(1)}, u32[]{:S(2)}, u32[]{:S(2)}) collective-permute-start(bf16[4,64,2048]{2,1,0:T(8,128)(2,1)} %collective-permute-done.2), channel_id=1, source_target_pairs={{0,1},{1,2},{2,3},{3,4},{4,5},{5,6},{6,7},{7,0},{8,9},{9,10},{10,1... | collective-permute-start | bytes 3145736 | tf_op jit(solution)/shard_map/ppermute | solution.py:25
  45.2 2.1 copy.39
  47.3 2.0 copy.40
  49.3 2.0 copy.41
  51.4 2.0 copy.42
  54.7 3.0 %collective-permute-start.5 = (bf16[4,64,2048]{2,1,0:T(8,128)(2,1)S(1)}, bf16[4,64,2048]{2,1,0:T(8,128)(2,1)S(1)}, u32[]{:S(2)}, u32[]{:S(2)}) collective-permute-start(bf16[4,64,2048]{2,1,0:T(8,128)(2,1)S(1)} %collective-permute-done.3), channel_id=1, source_target_pairs={{0,7},{1,0},{2,1},{3,2},{4,3},{5,4},{6,5},{7,6},{8,15},{9,8},{10,9... | collective-permute-start | bytes 3145736 | tf_op jit(solution)/shard_map/ppermute | solution.py:30
  57.7 2.3 %constant_dynamic-update-slice_fusion.6 = bf16[4,512,2048]{2,1,0:T(8,128)(2,1)} fusion(bf16[4,512,2048]{2,1,0:T(8,128)(2,1)} %get-tuple-element.161, bf16[4,64,2048]{2,1,0:T(8,128)(2,1)} %collective-permute-done, s32[]{:T(128)S(6)} %select_n.213), kind=kLoop, calls=%fused_computation.172 | loop fusion | bytes 2097156 | tf_op jit(solution)/shard_map/dynamic_update_slice | solution.py:26
  61.1 2.4 %constant_dynamic-update-slice_fusion.4 = bf16[4,512,2048]{2,1,0:T(8,128)(2,1)} fusion(bf16[4,512,2048]{2,1,0:T(8,128)(2,1)} %constant_dynamic-update-slice_fusion.5, bf16[4,64,2048]{2,1,0:T(8,128)(2,1)} %collective-permute-done.2, s32[]{:T(128)S(6)} %select_n.217), kind=kLoop, calls=%fused_computation.170 | loop fusion | bytes 2097156 | tf_op jit(solution)/shard_map/dynamic_update_slice | solution.py:26
  65.6 3.7 %collective-permute-done.5 = bf16[4,64,2048]{2,1,0:T(8,128)(2,1)S(1)} collective-permute-done((bf16[4,64,2048]{2,1,0:T(8,128)(2,1)S(1)}, bf16[4,64,2048]{2,1,0:T(8,128)(2,1)S(1)}, u32[]{:S(2)}, u32[]{:S(2)}) %collective-permute-start.5) | collective-permute-done | bytes 1048608 | tf_op jit(solution)/shard_map/ppermute | solution.py:30
  70.3 1.5 collective-permute-done.6
  72.8 9.7 %fusion.54 = bf16[4,512,512]{1,2,0:T(8,128)(2,1)S(1)} fusion(bf16[4,512,2048]{2,1,0:T(8,128)(2,1)} %constant_dynamic-update-slice_fusion, bf16[2048,128]{0,1:T(8,128)(2,1)S(1)} %copy-done.10, bf16[2048,128]{0,1:T(8,128)(2,1)S(1)} %copy-done.9, bf16[2048,128]{0,1:T(8,128)(2,1)S(1)} %copy-done.8, bf16[2048,128]{0,1:T(8,128)(2,1)S(1)} %copy-done.7), kind=kOutput, calls=%fused_computation.59 | convolution fusion | flops 4304404480 | bytes 12582912 | tf_op jit(solution)/shard_map/kux,xt->kut/dot_general | solution.py:149
  87.0 1.3 copy.44
  90.2 1.6 fusion.69
  91.8 11.9 %while.15 = (s32[]{:T(128)}, f32[4,1,128,128]{3,2,0,1:T(8,128)S(1)}, f32[4,4,1,128,128]{4,3,1,2,0:T(8,128)}, f32[1]{0:T(128)}, bf16[4,4,1,128,128]{4,3,1,2,0:T(8...) while((s32[]{:T(128)}, ...), condition=%wide.region_2.3_spmd.clone.clone.clone, body=%wide.region_1.2_spmd.clone.clone.clone.sunk | while | flops 67977728 | bytes 2496632 | solution.py:101
  106.0 8.3 %all-reduce = f32[4]{0:T(128)S(1)} all-reduce(f32[4]{0:T(128)S(1)} %exponential_dynamic-update-slice_fusion), channel_id=2, replica_groups=mesh['sp_0'=8,'sp_1'=4,'tp'=8] {'sp_1'}, use_global_device_ids=true, to_apply=%add | all-reduce | flops 4 | bytes 32
  116.8 18.0 %all-gather.8.cloned.1.call-done = f32[16,1,128,128]{3,2,1,0:T(8,128)} async-done(((f32[4,1,128,128]{3,2,1,0:T(8,128)}), f32[16,1,128,128]{3,2,1,0:T(8,128)}) %all-gather.8.cloned.1.call-update) | async-done | bytes 1048592 | tf_op jit(solution)/shard_map/all_gather | solution.py:48
  134.8 3.8 %slice_add_fusion.8 = f32[4,1,128,128]{3,2,1,0:T(8,128)} fusion(f32[16,1,128,128]{3,2,1,0:T(8,128)} %all-gather.8.cloned.1.call-done, f32[]{:T(128)} %bitcast.20, f32[]{:T(128)} %bitcast.18, f32[16,1,128,128]{3,2,0,1:T(8,128)} %bitcast.197, f32[]{:T(128)} %bitcast.16, f32[]{:T(128)} %bitcast.13), kind=kLoop, calls=%fused_computation.109 | loop fusion | flops 458752 | bytes 1310736 | tf_op jit(solution)/shard_map/add | solution.py:113
  139.3 1.4 dynamic-update-slice.1
  140.7 13.9 %all-reduce.1 = f32[8]{0:T(128)S(1)} all-reduce(f32[8]{0:T(128)S(1)} %dynamic-update-slice.1), channel_id=3, replica_groups=mesh['sp_0'=8,'sp_1'=4,'tp'=8] {'sp_0'}, use_global_device_ids=true, to_apply=%add.1 | all-reduce | flops 8 | bytes 64
  158.4 1.6 copy.48
  160.5 17.1 %all-gather.6.cloned.1.call-done = f32[8,4,1,128,128]{4,3,2,1,0:T(8,128)} async-done(((f32[1,4,1,128,128]{4,3,2,1,0:T(8,128)}), f32[8,4,1,128,128]{4,3,2,1,0:T(8,128)}) %all-gather.6.cloned.1.call-update) | async-done | bytes 2097168 | tf_op jit(solution)/shard_map/all_gather | solution.py:48
  177.6 7.8 %fusion.129 = (f32[4,512]{1,0:T(4,128)S(1)}, f32[4,512,128]{1,2,0:T(8,128)S(1)}) fusion(f32[4,512,128]{1,2,0:T(8,128)S(1)} %reshape.499, f32[8,4,1,128,128]{4,3,1,2,0:T(8,128)} %bitcast.204, f32[4,1,128,128]{3,2,1,0:T(8,128)S(1)} %copy-done.4, f32[16,1,128,128]{3,2,0,1:T(8,128)S(1)} %bitcast.198, f32[16,1,128,128]{3,2,1,0:T(8,128)S(1)} %copy-done.3, ...), kind=kOutput, calls=%fused_computation.183 | convolution fusion | flops 71170048 | bytes 5777468 | tf_op jit(solution)/shard_map/shld,shdv->shlv/dot_general | solution.py:122
  185.6 1.5 fusion.62
  187.4 18.6 %all_to_all.18 = bf16[4,512,128]{2,0,1:T(4,128)(2,1)S(1)} all-to-all(bf16[4,512,128]{2,0,1:T(4,128)(2,1)S(1)} %copy.65), channel_id=1, replica_groups=mesh['sp_0'=8,'sp_1'=4,'tp'=8] {'tp'}, dimensions={1} | all-to-all | bytes 1048576 | tf_op jit(solution)/shard_map/all_to_all | solution.py:180
  206.1 3.6 %multiply_reduce_fusion = (f32[4,64]{1,0:T(4,128)S(1)}, f32[4,64,2048]{2,1,0:T(8,128)S(1)}) fusion(bf16[1024,2048]{1,0:T(8,128)(2,1)} %param.20, bf16[4,8,8,8,128]{4,3,2,1,0:T(8,128)(2,1)S(1)} %bitcast.203), kind=kOutput, calls=%fused_computation.58 | convolution fusion | flops 1074790144 | bytes 6816768 | tf_op jit(solution)/shard_map/hor,rn->hon/dot_general | solution.py:178
  (102 shorter events, 33.7 us)
Async XLA Ops:
  6.5 128.2 %all-gather.8.cloned.1.call-start = ((), (), s32[]{:S(2)}) async-start(), calls=%async_computation.2 | async-start | bytes 1310720 | tf_op jit(solution)/shard_map/all_gather | solution.py:48
  8.1 4.3 %copy-start.1 = (bf16[4,64,2048]{2,1,0:T(8,128)(2,1)S(1)}, bf16[4,64,2048]{2,1,0:T(8,128)(2,1)}, u32[]{:S(2)}) copy-start(bf16[4,64,2048]{2,1,0:T(8,128)(2,1)} %param.12) | copy-start | bytes 3145732
  8.1 4.3 %copy-start.11 = (f32[2048]{0:T(1024)S(1)}, f32[2048]{0:T(1024)}, u32[]{:S(2)}) copy-start(f32[2048]{0:T(1024)} %param.13) | copy-start | bytes 24580
  13.7 14.4 %collective-permute-start = (bf16[4,64,2048]{2,1,0:T(8,128)(2,1)S(1)}, bf16[4,64,2048]{2,1,0:T(8,128)(2,1)}, u32[]{:S(2)}, u32[]{:S(2)}) collective-permute-start(bf16[4,64,2048]{2,1,0:T(8,128)(2,1)S(1)} %get-tuple-element.162), channel_id=1, source_target_pairs={{0,1},{1,2},{2,3},{3,4},{4,5},{5,6},{6,7},{7,0},{8,9},{9,10},{10,1... | collective-permute-start | bytes 3145736 | tf_op jit(solution)/shard_map/ppermute | solution.py:25
  16.3 14.6 %collective-permute-start.1 = (bf16[4,64,2048]{2,1,0:T(8,128)(2,1)S(1)}, bf16[4,64,2048]{2,1,0:T(8,128)(2,1)S(1)}, u32[]{:S(2)}, u32[]{:S(2)}) collective-permute-start(bf16[4,64,2048]{2,1,0:T(8,128)(2,1)S(1)} %get-tuple-element.162), channel_id=1, source_target_pairs={{0,7},{1,0},{2,1},{3,2},{4,3},{5,4},{6,5},{7,6},{8,15},{9,8},{10,9... | collective-permute-start | bytes 3145736 | tf_op jit(solution)/shard_map/ppermute | solution.py:30
  28.1 14.6 %collective-permute-start.2 = (bf16[4,64,2048]{2,1,0:T(8,128)(2,1)}, bf16[4,64,2048]{2,1,0:T(8,128)(2,1)}, u32[]{:S(2)}, u32[]{:S(2)}) collective-permute-start(bf16[4,64,2048]{2,1,0:T(8,128)(2,1)} %collective-permute-done), channel_id=1, source_target_pairs={{0,1},{1,2},{2,3},{3,4},{4,5},{5,6},{6,7},{7,0},{8,9},{9,10},{10,1... | collective-permute-start | bytes 3145736 | tf_op jit(solution)/shard_map/ppermute | solution.py:25
  30.9 23.8 %collective-permute-start.3 = (bf16[4,64,2048]{2,1,0:T(8,128)(2,1)S(1)}, bf16[4,64,2048]{2,1,0:T(8,128)(2,1)S(1)}, u32[]{:S(2)}, u32[]{:S(2)}) collective-permute-start(bf16[4,64,2048]{2,1,0:T(8,128)(2,1)S(1)} %collective-permute-done.1), channel_id=1, source_target_pairs={{0,7},{1,0},{2,1},{3,2},{4,3},{5,4},{6,5},{7,6},{8,15},{9,8},{10,9... | collective-permute-start | bytes 3145736 | tf_op jit(solution)/shard_map/ppermute | solution.py:30
  42.7 17.3 %collective-permute-start.4 = (bf16[4,64,2048]{2,1,0:T(8,128)(2,1)}, bf16[4,64,2048]{2,1,0:T(8,128)(2,1)S(1)}, u32[]{:S(2)}, u32[]{:S(2)}) collective-permute-start(bf16[4,64,2048]{2,1,0:T(8,128)(2,1)} %collective-permute-done.2), channel_id=1, source_target_pairs={{0,1},{1,2},{2,3},{3,4},{4,5},{5,6},{6,7},{7,0},{8,9},{9,10},{10,1... | collective-permute-start | bytes 3145736 | tf_op jit(solution)/shard_map/ppermute | solution.py:25
  54.7 14.5 %collective-permute-start.5 = (bf16[4,64,2048]{2,1,0:T(8,128)(2,1)S(1)}, bf16[4,64,2048]{2,1,0:T(8,128)(2,1)S(1)}, u32[]{:S(2)}, u32[]{:S(2)}) collective-permute-start(bf16[4,64,2048]{2,1,0:T(8,128)(2,1)S(1)} %collective-permute-done.3), channel_id=1, source_target_pairs={{0,7},{1,0},{2,1},{3,2},{4,3},{5,4},{6,5},{7,6},{8,15},{9,8},{10,9... | collective-permute-start | bytes 3145736 | tf_op jit(solution)/shard_map/ppermute | solution.py:30
  60.0 11.7 %collective-permute-start.6 = (bf16[4,64,2048]{2,1,0:T(8,128)(2,1)S(1)}, bf16[4,64,2048]{2,1,0:T(8,128)(2,1)S(1)}, u32[]{:S(2)}, u32[]{:S(2)}) collective-permute-start(bf16[4,64,2048]{2,1,0:T(8,128)(2,1)S(1)} %collective-permute-done.4), channel_id=1, source_target_pairs={{0,1},{1,2},{2,3},{3,4},{4,5},{5,6},{6,7},{7,0},{8,9},{9,10},{10,1... | collective-permute-start | bytes 3145736 | tf_op jit(solution)/shard_map/ppermute | solution.py:25
  63.4 9.4 %copy-start.7 = (bf16[2048,128]{0,1:T(8,128)(2,1)S(1)}, bf16[2048,128]{0,1:T(8,128)(2,1)}, u32[]{:S(2)}) copy-start(bf16[2048,128]{0,1:T(8,128)(2,1)} %copy.39) | copy-start | bytes 1572868
  63.4 9.4 %copy-start.8 = (bf16[2048,128]{0,1:T(8,128)(2,1)S(1)}, bf16[2048,128]{0,1:T(8,128)(2,1)}, u32[]{:S(2)}) copy-start(bf16[2048,128]{0,1:T(8,128)(2,1)} %copy.40) | copy-start | bytes 1572868
  63.5 9.4 %copy-start.9 = (bf16[2048,128]{0,1:T(8,128)(2,1)S(1)}, bf16[2048,128]{0,1:T(8,128)(2,1)}, u32[]{:S(2)}) copy-start(bf16[2048,128]{0,1:T(8,128)(2,1)} %copy.41) | copy-start | bytes 1572868
  63.5 9.4 %copy-start.10 = (bf16[2048,128]{0,1:T(8,128)(2,1)S(1)}, bf16[2048,128]{0,1:T(8,128)(2,1)}, u32[]{:S(2)}) copy-start(bf16[2048,128]{0,1:T(8,128)(2,1)} %copy.42) | copy-start | bytes 1572868
  82.5 1.3 copy-start.2
  85.0 0.7 copy-start.5
  85.0 0.8 copy-start.6
  91.7 12.8 %copy-start.15 = (u32[256]{0:T(256)S(1)}, u32[256]{0:T(256)}, u32[]{:S(2)}) copy-start(u32[256]{0:T(256)} %constant.135) | copy-start | bytes 3076
  91.8 46.9 %copy-start.14 = (u32[256]{0:T(256)S(1)}, u32[256]{0:T(256)}, u32[]{:S(2)}) copy-start(u32[256]{0:T(256)} %constant.140) | copy-start | bytes 3076
  103.7 0.7 copy-start
  104.4 73.2 %all-gather.6.cloned.1.call-start = ((), (), s32[]{:S(2)}) async-start(), calls=%async_computation.1 | async-start | bytes 2359296 | tf_op jit(solution)/shard_map/all_gather | solution.py:48
  134.8 42.9 %copy-start.3 = (f32[16,1,128,128]{3,2,1,0:T(8,128)S(1)}, f32[16,1,128,128]{3,2,1,0:T(8,128)}, u32[]{:S(2)}) copy-start(f32[16,1,128,128]{3,2,1,0:T(8,128)} %all-gather.8.cloned.1.call-done) | copy-start | bytes 3145732
  138.6 39.0 %copy-start.4 = (f32[4,1,128,128]{3,2,1,0:T(8,128)S(1)}, f32[4,1,128,128]{3,2,1,0:T(8,128)}, u32[]{:S(2)}) copy-start(f32[4,1,128,128]{3,2,1,0:T(8,128)} %slice_add_fusion.8) | copy-start | bytes 786436
  160.1 25.5 %copy-start.13 = (f32[128]{0:T(128)S(1)}, f32[128]{0:T(128)}, u32[]{:S(2)}) copy-start(f32[128]{0:T(128)} %param.19) | copy-start | bytes 1540
  206.0 3.7 %copy-start.12 = (f32[2048]{0:T(1024)S(1)}, f32[2048]{0:T(1024)}, u32[]{:S(2)}) copy-start(f32[2048]{0:T(1024)} %param.21) | copy-start | bytes 24580
Sparse Core Ops, SparseCore 0:
  104.6 30.1 all-gather.7
  138.8 38.8 all-gather.5
